TPU v7x, 32 devices: a whole 2x2x4 slice. The times are simulated.
32 devices in a mesh: sp: 8 (over y, x, core), tp: 4 (over z).
Axes of the slice: x: 2, y: 2, z: 4, core: 2. Of those that a mesh axis runs over, the one named last changes fastest.
Arguments:
- sequence: bfloat16 [4, 256, 1024], P(None, 'sp', 'tp'), may hold values from -6 to 6
- norm_gain: float32 [3, 1024], replicated, may hold values from 0.1 to 1.9
- weight_value: bfloat16 [3, 1024, 512], P(None, 'sp', 'tp'), may hold values from -0.1875 to 0.1875
- weight_outer: bfloat16 [3, 1024, 512], P(None, 'sp', 'tp'), may hold values from -0.1875 to 0.1875
- weight_inner: bfloat16 [3, 1024, 512], P(None, 'sp', 'tp'), may hold values from -0.1875 to 0.1875
- conv_taps: float32 [3, 3, 512], P(None, None, 'tp'), may hold values from -3 to 3
- weight_out: bfloat16 [3, 512, 1024], P(None, 'tp', 'sp'), may hold values from -0.25 to 0.25
Outputs:
- mixed: bfloat16 [4, 256, 1024], P(None, 'sp', 'tp')
All inputs are finite; a program needn't handle non-finite values.
Results may differ from a plain program's by a relative error of at most 0.03.
Values may be sent and summed in bfloat16 or wider, within the bound.
A program may use at most 64 MiB of HBM per device.

v0:
```python
import jax
import jax.numpy as jnp
from jax import lax
from jax.sharding import PartitionSpec as P

LAYERS = 3


def folded(array, axis, dim, update, carry):
    whole = jax.tree.map(lambda part: lax.all_gather(part, axis, axis=dim, tiled=True), array)
    return update(carry, whole, jnp.int32(0))


def from_behind(value, axis, steps):
    count = lax.axis_size(axis)
    first, last = max(0, -steps), min(count, count - steps)
    return lax.ppermute(value, axis, [(source, source + steps) for source in range(first, last)])


def over_all(slab, axis, dim, apply):
    everything = lax.all_gather(slab, axis, axis=dim, tiled=True)
    return apply(everything, jnp.int32(0))


def rms_rows(values, gain_row):
    wide = values.astype(jnp.float32)
    scaled = wide * lax.rsqrt(jnp.mean(wide * wide, axis=-1, keepdims=True) + 1e-06)
    return (scaled * gain_row).astype(jnp.bfloat16)


def body(sequence, norm_gain, weight_value, weight_outer, weight_inner, conv_taps, weight_out):
    current = sequence
    seq_count = sequence.shape[0]
    local_len = sequence.shape[1]
    channels = weight_value.shape[2]
    depth = conv_taps.shape[1]
    for layer_index in range(LAYERS):
        whole = lax.all_gather(current, "tp", axis=2, tiled=True)
        normed = rms_rows(whole, norm_gain[layer_index]).reshape(
            seq_count * local_len, whole.shape[2]
        )
        empty = jnp.zeros((normed.shape[0], channels), jnp.float32)

        def add_rows(running, weight_rows, offset):
            columns = lax.dynamic_slice_in_dim(normed, offset, weight_rows.shape[0], 1)
            return running + jnp.dot(columns, weight_rows, preferred_element_type=jnp.float32)

        sum_value = folded(weight_value[layer_index], "sp", 0, add_rows, empty)
        sum_outer = folded(weight_outer[layer_index], "sp", 0, add_rows, empty)
        sum_inner = folded(weight_inner[layer_index], "sp", 0, add_rows, empty)
        proj_value = sum_value.astype(jnp.bfloat16)
        proj_outer = sum_outer.astype(jnp.bfloat16)
        proj_inner = sum_inner.astype(jnp.bfloat16)
        product = (proj_inner.astype(jnp.float32) * proj_value.astype(jnp.float32)).reshape(
            seq_count, local_len, channels
        )
        last_rows = product[:, local_len - (depth - 1) :, :]
        before = from_behind(last_rows, "sp", 1)
        padded = jnp.concatenate([before, product], axis=1)
        filtered = conv_taps[layer_index, 0] * padded[:, 0:local_len]
        for offset in range(1, depth):
            filtered = (
                filtered + conv_taps[layer_index, offset] * padded[:, offset : offset + local_len]
            )
        gated = (
            proj_outer.astype(jnp.float32).reshape(seq_count, local_len, channels) * filtered
        ).astype(jnp.bfloat16)
        gated_rows = gated.reshape(seq_count * local_len, channels)

        def project_columns(weight_cols, offset):
            return jnp.dot(gated_rows, weight_cols, preferred_element_type=jnp.float32)

        terms = over_all(weight_out[layer_index], "sp", 1, project_columns)
        shares = lax.psum_scatter(
            terms.astype(jnp.bfloat16), "tp", scatter_dimension=1, tiled=True
        ).astype(jnp.float32)
        shares = shares.reshape(seq_count, local_len, shares.shape[1])
        current = (current.astype(jnp.float32) + shares).astype(jnp.bfloat16)
    return current


def solution(mesh):
    return jax.shard_map(
        body,
        mesh=mesh,
        in_specs=(
            P(None, "sp", "tp"),
            P(),
            P(None, "sp", "tp"),
            P(None, "sp", "tp"),
            P(None, "sp", "tp"),
            P(None, None, "tp"),
            P(None, "tp", "sp"),
        ),
        out_specs=P(None, "sp", "tp"),
        check_vma=False,
    )
```

profile of v0, /device:TPU:0, one launch (start us, length us, event | category | flops | bytes accessed | tf_op | source)
XLA Modules:
  0.0 209.8 jit_solution(15252150934710512580)
XLA Ops:
  7.4 15.7 %all_gather.45 = bf16[4,32,1024]{2,1,0:T(8,128)(2,1)S(1)} all-gather(bf16[4,32,256]{2,1,0:T(8,128)(2,1)} %param.7), channel_id=1, replica_groups=mesh['sp'=8,'tp'=4] {'tp'}, dimensions={2}, use_global_device_ids=true | all-gather | bytes 327680 | tf_op jit(solution)/shard_map/all_gather | solution.py:38
  24.0 9.4 %all-gather.1 = bf16[1,1024,128]{2,1,0:T(8,128)(2,1)S(1)} all-gather(bf16[1,128,128]{2,1,0:T(8,128)(2,1)S(1)} %get-tuple-element.15), channel_id=3, replica_groups=mesh['sp'=8,'tp'=4] {'sp'}, dimensions={1}, use_global_device_ids=true | all-gather | bytes 294912 | tf_op jit(solution)/shard_map/all_gather | solution.py:10
  33.5 9.3 %all-gather.2 = bf16[1,1024,128]{2,1,0:T(8,128)(2,1)S(1)} all-gather(bf16[1,128,128]{2,1,0:T(8,128)(2,1)S(1)} %get-tuple-element.12), channel_id=4, replica_groups=mesh['sp'=8,'tp'=4] {'sp'}, dimensions={1}, use_global_device_ids=true | all-gather | bytes 294912 | tf_op jit(solution)/shard_map/all_gather | solution.py:10
  43.4 2.3 %collective-permute-start = (f32[4,2,128]{2,1,0:T(2,128)S(1)}, f32[4,2,128]{2,1,0:T(2,128)S(1)}, u32[]{:S(2)}, u32[]{:S(2)}) collective-permute-start(f32[4,2,128]{2,1,0:T(2,128)S(1)} %slice.132), channel_id=1, source_target_pairs={{0,4},{4,8},{8,12},{12,16},{16,20},{20,24},{24,28},{1,5},{5,9},{9,... | collective-permute-start | bytes 12296 | tf_op jit(solution)/shard_map/ppermute | solution.py:17
  45.7 8.3 %all-gather = bf16[1,1024,128]{2,1,0:T(8,128)(2,1)S(1)} all-gather(bf16[1,128,128]{2,1,0:T(8,128)(2,1)S(1)} %get-tuple-element.9), channel_id=2, replica_groups=mesh['sp'=8,'tp'=4] {'sp'}, dimensions={1}, use_global_device_ids=true | all-gather | bytes 294912 | tf_op jit(solution)/shard_map/all_gather | solution.py:10
  54.9 9.3 %all-gather.3 = bf16[1,128,1024]{2,1,0:T(8,128)(2,1)S(1)} all-gather(bf16[1,128,128]{2,1,0:T(8,128)(2,1)S(1)} %get-tuple-element.6), channel_id=5, replica_groups=mesh['sp'=8,'tp'=4] {'sp'}, dimensions={2}, use_global_device_ids=true | all-gather | bytes 294912 | tf_op jit(solution)/shard_map/all_gather | solution.py:21
  64.3 0.9 convolution_convert_fusion.2
  65.3 8.3 %all-gather.5 = bf16[1,1024,128]{2,1,0:T(8,128)(2,1)S(1)} all-gather(bf16[1,128,128]{2,1,0:T(8,128)(2,1)S(1)} %get-tuple-element.16), channel_id=7, replica_groups=mesh['sp'=8,'tp'=4] {'sp'}, dimensions={1}, use_global_device_ids=true | all-gather | bytes 294912 | tf_op jit(solution)/shard_map/all_gather | solution.py:10
  73.6 9.3 %all-gather.6 = bf16[1,1024,128]{2,1,0:T(8,128)(2,1)S(1)} all-gather(bf16[1,128,128]{2,1,0:T(8,128)(2,1)S(1)} %get-tuple-element.13), channel_id=8, replica_groups=mesh['sp'=8,'tp'=4] {'sp'}, dimensions={1}, use_global_device_ids=true | all-gather | bytes 294912 | tf_op jit(solution)/shard_map/all_gather | solution.py:10
  82.9 8.3 %all-gather.4 = bf16[1,1024,128]{2,1,0:T(8,128)(2,1)S(1)} all-gather(bf16[1,128,128]{2,1,0:T(8,128)(2,1)S(1)} %get-tuple-element.10), channel_id=6, replica_groups=mesh['sp'=8,'tp'=4] {'sp'}, dimensions={1}, use_global_device_ids=true | all-gather | bytes 294912 | tf_op jit(solution)/shard_map/all_gather | solution.py:10
  91.2 9.5 %all-gather.7 = bf16[1,128,1024]{2,1,0:T(8,128)(2,1)S(1)} all-gather(bf16[1,128,128]{2,1,0:T(8,128)(2,1)S(1)} %get-tuple-element.7), channel_id=9, replica_groups=mesh['sp'=8,'tp'=4] {'sp'}, dimensions={2}, use_global_device_ids=true | all-gather | bytes 294912 | tf_op jit(solution)/shard_map/all_gather | solution.py:21
  100.7 0.9 fusion.32
  101.5 14.5 %all_gather.50 = bf16[4,32,1024]{2,1,0:T(8,128)(2,1)S(1)} all-gather(bf16[4,32,256]{2,1,0:T(8,128)(2,1)S(1)} %fusion.32), channel_id=1, replica_groups=mesh['sp'=8,'tp'=4] {'tp'}, dimensions={2}, use_global_device_ids=true | all-gather | bytes 327680 | tf_op jit(solution)/shard_map/all_gather | solution.py:38
  116.8 1.3 collective-permute-start.1
  119.0 0.9 convolution_convert_fusion.1
  119.9 12.0 %all-gather.9 = bf16[1,1024,128]{2,1,0:T(8,128)(2,1)S(1)} all-gather(bf16[1,128,128]{2,1,0:T(8,128)(2,1)S(1)} %get-tuple-element.14), channel_id=11, replica_groups=mesh['sp'=8,'tp'=4] {'sp'}, dimensions={1}, use_global_device_ids=true | all-gather | bytes 294912 | tf_op jit(solution)/shard_map/all_gather | solution.py:10
  132.0 8.4 %all-gather.10 = bf16[1,1024,128]{2,1,0:T(8,128)(2,1)S(1)} all-gather(bf16[1,128,128]{2,1,0:T(8,128)(2,1)S(1)} %get-tuple-element.11), channel_id=12, replica_groups=mesh['sp'=8,'tp'=4] {'sp'}, dimensions={1}, use_global_device_ids=true | all-gather | bytes 294912 | tf_op jit(solution)/shard_map/all_gather | solution.py:10
  140.4 9.2 %all-gather.8 = bf16[1,1024,128]{2,1,0:T(8,128)(2,1)S(1)} all-gather(bf16[1,128,128]{2,1,0:T(8,128)(2,1)S(1)} %get-tuple-element.8), channel_id=10, replica_groups=mesh['sp'=8,'tp'=4] {'sp'}, dimensions={1}, use_global_device_ids=true | all-gather | bytes 294912 | tf_op jit(solution)/shard_map/all_gather | solution.py:10
  149.6 8.4 %all-gather.11 = bf16[1,128,1024]{2,1,0:T(8,128)(2,1)S(1)} all-gather(bf16[1,128,128]{2,1,0:T(8,128)(2,1)S(1)} %get-tuple-element.5), channel_id=13, replica_groups=mesh['sp'=8,'tp'=4] {'sp'}, dimensions={2}, use_global_device_ids=true | all-gather | bytes 294912 | tf_op jit(solution)/shard_map/all_gather | solution.py:21
  158.9 14.5 %all_gather.55 = bf16[4,32,1024]{2,1,0:T(8,128)(2,1)S(1)} all-gather(bf16[4,32,256]{2,1,0:T(8,128)(2,1)S(1)} %fusion.31), channel_id=1, replica_groups=mesh['sp'=8,'tp'=4] {'tp'}, dimensions={2}, use_global_device_ids=true | all-gather | bytes 327680 | tf_op jit(solution)/shard_map/all_gather | solution.py:38
  174.2 1.3 collective-permute-start.2
  176.3 0.9 convolution_convert_fusion
  177.2 24.6 %reduce-scatter.8.cloned.1.call-done = bf16[128,256]{1,0:T(8,128)(2,1)} async-done(((bf16[128,1024]{1,0:T(8,128)(2,1)}), bf16[128,256]{1,0:T(8,128)(2,1)}) %reduce-scatter.8.cloned.1.call-update) | async-done | bytes 65552 | tf_op jit(solution)/shard_map/reduce_scatter | solution.py:74
  201.8 1.5 fusion.30
  (54 shorter events, 7.4 us)
Async XLA Ops:
  6.5 94.1 %reduce-scatter.4.cloned.1.call-start = ((), (), s32[]{:S(2)}) async-start(), calls=%async_computation.3 | async-start | bytes 327680 | tf_op jit(solution)/shard_map/reduce_scatter | solution.py:74
  23.1 0.9 copy-start.1
  24.0 9.5 %copy-start.2 = (bf16[3,128,128]{2,1,0:T(8,128)(2,1)S(1)}, bf16[3,128,128]{2,1,0:T(8,128)(2,1)}, u32[]{:S(2)}) copy-start(bf16[3,128,128]{2,1,0:T(8,128)(2,1)} %param.9) | copy-start | bytes 294916
  43.1 2.5 %copy-start.3 = (bf16[3,128,128]{2,1,0:T(8,128)(2,1)S(1)}, bf16[3,128,128]{2,1,0:T(8,128)(2,1)}, u32[]{:S(2)}) copy-start(bf16[3,128,128]{2,1,0:T(8,128)(2,1)} %param.10) | copy-start | bytes 294916
  43.4 20.9 %collective-permute-start = (f32[4,2,128]{2,1,0:T(2,128)S(1)}, f32[4,2,128]{2,1,0:T(2,128)S(1)}, u32[]{:S(2)}, u32[]{:S(2)}) collective-permute-start(f32[4,2,128]{2,1,0:T(2,128)S(1)} %slice.132), channel_id=1, source_target_pairs={{0,4},{4,8},{8,12},{12,16},{16,20},{20,24},{24,28},{1,5},{5,9},{9,... | collective-permute-start | bytes 12296 | tf_op jit(solution)/shard_map/ppermute | solution.py:17
  54.0 0.7 copy-start.5
  54.0 0.9 copy-start.4
  65.2 92.8 %reduce-scatter.6.cloned.1.call-start = ((), (), s32[]{:S(2)}) async-start(), calls=%async_computation.4 | async-start | bytes 327680 | tf_op jit(solution)/shard_map/reduce_scatter | solution.py:74
  91.2 9.5 %copy-start = (bf16[4,32,256]{2,1,0:T(8,128)(2,1)S(1)}, bf16[4,32,256]{2,1,0:T(8,128)(2,1)}, u32[]{:S(2)}) copy-start(bf16[4,32,256]{2,1,0:T(8,128)(2,1)} %param.7) | copy-start | bytes 196612
  116.8 2.1 %collective-permute-start.1 = (f32[4,2,128]{2,1,0:T(2,128)S(1)}, f32[4,2,128]{2,1,0:T(2,128)S(1)}, u32[]{:S(2)}, u32[]{:S(2)}) collective-permute-start(f32[4,2,128]{2,1,0:T(2,128)S(1)} %slice.135), channel_id=1, source_target_pairs={{0,4},{4,8},{8,12},{12,16},{16,20},{20,24},{24,28},{1,5},{5,9},{9,... | collective-permute-start | bytes 12296 | tf_op jit(solution)/shard_map/ppermute | solution.py:17
  119.9 81.9 %reduce-scatter.8.cloned.1.call-start = ((), (), s32[]{:S(2)}) async-start(), calls=%async_computation.5 | async-start | bytes 327680 | tf_op jit(solution)/shard_map/reduce_scatter | solution.py:74
  174.2 2.1 %collective-permute-start.2 = (f32[4,2,128]{2,1,0:T(2,128)S(1)}, f32[4,2,128]{2,1,0:T(2,128)S(1)}, u32[]{:S(2)}, u32[]{:S(2)}) collective-permute-start(f32[4,2,128]{2,1,0:T(2,128)S(1)} %slice.138), channel_id=1, source_target_pairs={{0,4},{4,8},{8,12},{12,16},{16,20},{20,24},{24,28},{1,5},{5,9},{9,... | collective-permute-start | bytes 12296 | tf_op jit(solution)/shard_map/ppermute | solution.py:17
Sparse Core Ops, SparseCore 0:
  65.4 20.6 reduce-scatter.3
  120.0 23.5 reduce-scatter.5
  177.4 24.3 reduce-scatter.7
where the time goes:
time: 211 us; the launch traced here: 210 us
  blocking collectives  155 us (73%)
  waiting for transfers between devices  25.8 us (12%)
  between operations  13.3 us (6%)
  starting transfers between devices  4.92 us (2%)
  matrix products  4.74 us (2%)
  other arithmetic  4.12 us (2%)
  local copies, waits for them, and re-layouts  2.34 us (1%)
    all_gather x9, blocking collectives, folded(): lax.all_gather(part, axis, axis=dim, tiled=True)  82.6 us
    all_gather x3, blocking collectives, body(): whole = lax.all_gather(current, 'tp', axis=2, tiled=True)  44.8 us
    all_gather x3, blocking collectives, over_all(): everything = lax.all_gather(slab, axis, axis=dim, tiled=True)  27.2 us
    reduce_scatter x3, waiting for transfers between devices, body(): lax.psum_scatter(terms.astype(jnp.bfloat16), 'tp', scatter_dimension=1, t...  24.6 us
    ppermute x3, starting transfers between devices, from_behind(): lax.ppermute(value, axis, [(source, source + steps) for source in range(f...  4.83 us
  transfers between devices with their start and end apart: 6, of which 3 were waited for; matrix products, arithmetic and copies ran while one was open for 0% of the time, Pallas kernels for 0%

commit v1 on v0

--- a/solution.py
+++ b/solution.py
@@ -1,6 +1,10 @@
+import functools
+
 import jax
 import jax.numpy as jnp
 from jax import lax
+from jax.experimental import pallas as pl
+from jax.experimental.pallas import tpu as pltpu
 from jax.sharding import PartitionSpec as P
 
 LAYERS = 3
@@ -79,9 +83,259 @@
     return current
 
 
+CORES = 2
+HALO = 8
+HALO_SENT = 16
+COPIES = 176
+MESH = pl.DeviceIdType.MESH
+
+
+def kernel(
+    sp, tp, seq_ref, gain_ref, value_ref, outer_ref, inner_ref, taps_ref, out_w_ref, mixed_ref,
+    main, edge, win, wout, gates, current,
+    send_sem, local_sem, seq_sem, edge_sem, win_sem, win_own_sem, win_fwd_sem,
+    rows_sem, wout_sem, wout_own_sem, wout_fwd_sem, gate_sem,
+):
+    s, t = lax.axis_index("sp"), lax.axis_index("tp")
+    chips = sp // CORES
+    chip, core = s // CORES, s % CORES
+    partner = chip * CORES + (CORES - 1 - core)
+    seqs, length, feats = seq_ref.shape
+    layers, depth_w, channels = value_ref.shape
+    taps = taps_ref.shape[1]
+    rows = seqs * (HALO + length)
+    width = feats * tp
+    sources = (value_ref, outer_ref, inner_ref)
+    sends, locals_ = [], []
+
+    def at(sp_index, tp_index):
+        return {"sp": sp_index, "tp": tp_index}
+
+    def along(step):
+        return lax.rem(t + step + tp, tp)
+
+    def peer(step):
+        return lax.rem(chip + step + chips, chips) * CORES + core
+
+    def remote(src, dst, recv, device):
+        copy = pltpu.make_async_remote_copy(
+            src_ref=src, dst_ref=dst, send_sem=send_sem.at[len(sends)], recv_sem=recv,
+            device_id=device, device_id_type=MESH,
+        )
+        copy.start()
+        sends.append(copy)
+
+    def arrived(dst, recv):
+        pltpu.make_async_remote_copy(
+            src_ref=dst, dst_ref=dst, send_sem=send_sem.at[0], recv_sem=recv,
+            device_id=at(partner, t), device_id_type=MESH,
+        ).wait_recv()
+
+    def local(src, dst):
+        copy = pltpu.make_async_copy(src, dst, local_sem.at[len(locals_)])
+        copy.start()
+        locals_.append(copy)
+        return copy
+
+    right, left = lax.rem(s + 1, sp), lax.rem(s + sp - 1, sp)
+    greeted = [at(s, along(step)) for step in range(1, tp)]
+    greeted += [at(peer(step), t) for step in range(1, chips)]
+    greeted += [at(partner, t)]
+    greeted += [at(side, along(step)) for side in (left, right) for step in range(tp)]
+    barrier = pltpu.get_barrier_semaphore()
+    for device in greeted:
+        pl.semaphore_signal(barrier, inc=1, device_id=device, device_id_type=MESH)
+    own_main = local(seq_ref, main.at[t])
+    own_in = [[local(ref.at[l], win.at[l, s, k]) for k, ref in enumerate(sources)] for l in range(layers)]
+    own_out = [local(out_w_ref.at[l], wout.at[l, s, t]) for l in range(layers)]
+    pl.semaphore_wait(barrier, len(greeted))
+
+    def send_in(l):
+        for k, ref in enumerate(sources):
+            for step in range(1, chips):
+                remote(ref.at[l], win.at[l, s, k], win_sem.at[l, step, k], at(peer(step), t))
+            remote(ref.at[l], win.at[l, s, k], win_own_sem.at[l, k], at(partner, t))
+
+    def send_rows(l):
+        for step in range(1, tp):
+            remote(out_w_ref.at[l], wout.at[l, s, t], rows_sem.at[l, step], at(s, along(step)))
+
+    def forward_in(l):
+        for step in range(1, chips):
+            origin = peer(-step)
+            for k in range(len(sources)):
+                arrived(win.at[l, origin, k], win_sem.at[l, step, k])
+            remote(win.at[l, origin], win.at[l, origin], win_fwd_sem.at[l, step], at(partner, t))
+
+    def spread_out(l):
+        own_out[l].wait()
+        for step in range(1, tp):
+            arrived(wout.at[l, s, along(-step)], rows_sem.at[l, step])
+        for step in range(1, chips):
+            remote(wout.at[l, s], wout.at[l, s], wout_sem.at[l, step], at(peer(step), t))
+        remote(wout.at[l, s], wout.at[l, s], wout_own_sem.at[l], at(partner, t))
+
+    def forward_out(l):
+        for step in range(1, chips):
+            origin = peer(-step)
+            arrived(wout.at[l, origin], wout_sem.at[l, step])
+            remote(wout.at[l, origin], wout.at[l, origin], wout_fwd_sem.at[l, step], at(partner, t))
+
+    def finish_in(l):
+        for copy in own_in[l]:
+            copy.wait()
+        for k in range(len(sources)):
+            arrived(win.at[l, partner, k], win_own_sem.at[l, k])
+        for step in range(1, chips):
+            origin = lax.rem(chip - step + chips, chips) * CORES + (CORES - 1 - core)
+            arrived(win.at[l, origin], win_fwd_sem.at[l, step])
+
+    def finish_out(l):
+        arrived(wout.at[l, partner], wout_own_sem.at[l])
+        for step in range(1, chips):
+            origin = lax.rem(chip - step + chips, chips) * CORES + (CORES - 1 - core)
+            arrived(wout.at[l, origin], wout_fwd_sem.at[l, step])
+
+    def gate_layer(l):
+        wide = current[...]
+        scaled = wide * lax.rsqrt(jnp.mean(wide * wide, axis=-1, keepdims=True) + 1e-06)
+        normed = (scaled * gain_ref[l : l + 1, :]).astype(jnp.bfloat16)
+        finish_in(l)
+        weights = jnp.concatenate(
+            [win[l, :, k].reshape(width, channels) for k in range(len(sources))], axis=1
+        )
+        proj = jnp.dot(normed, weights, preferred_element_type=jnp.float32)
+        proj = proj.astype(jnp.bfloat16).astype(jnp.float32)
+        product = proj[:, 2 * channels :] * proj[:, :channels]
+        filtered = taps_ref[l, taps - 1 : taps, :] * product
+        for back in range(1, taps):
+            shifted = jnp.concatenate(
+                [jnp.zeros((back, channels), jnp.float32), product[: rows - back]], axis=0
+            )
+            filtered = filtered + taps_ref[l, taps - 1 - back : taps - back, :] * shifted
+        gates[l, t] = (proj[:, channels : 2 * channels] * filtered).astype(jnp.bfloat16)
+        for step in range(1, tp):
+            remote(gates.at[l, t], gates.at[l, t], gate_sem.at[l, step], at(s, along(step)))
+
+    def all_gates(l):
+        for step in range(1, tp):
+            arrived(gates.at[l, along(-step)], gate_sem.at[l, step])
+        return jnp.concatenate([gates[l, j] for j in range(tp)], axis=1)
+
+    for step in range(1, tp):
+        remote(seq_ref, main.at[t], seq_sem.at[step], at(s, along(step)))
+    for step in range(tp):
+        remote(
+            seq_ref.at[:, pl.ds(length - HALO_SENT, HALO_SENT), :], edge.at[t], edge_sem.at[step],
+            at(right, along(step)),
+        )
+    send_in(0)
+    for l in range(layers):
+        send_rows(l)
+    send_in(1)
+    forward_in(0)
+    spread_out(0)
+    own_main.wait()
+    for step in range(1, tp):
+        arrived(main.at[along(-step)], seq_sem.at[step])
+    for step in range(tp):
+        arrived(edge.at[along(-step)], edge_sem.at[step])
+    inside = jnp.where(s == 0, 0.0, 1.0).astype(jnp.float32)
+    for j in range(tp):
+        before = edge[j].astype(jnp.float32)[:, HALO_SENT - HALO :, :] * inside
+        both = jnp.concatenate([before, main[j].astype(jnp.float32)], axis=1)
+        current[:, j * feats : (j + 1) * feats] = both.reshape(rows, feats)
+
+    per_dot = 2
+    for l in range(layers):
+        gate_layer(l)
+        if l + 2 < layers:
+            send_in(l + 2)
+        if l + 1 < layers:
+            forward_in(l + 1)
+            spread_out(l + 1)
+        forward_out(l)
+        gated = all_gates(l)
+        finish_out(l)
+
+        def columns(first):
+            return jnp.concatenate(
+                [wout[l, first + j].reshape(tp * channels, depth_w) for j in range(per_dot)], axis=1
+            )
+
+        if l < layers - 1:
+            for first in range(0, sp, per_dot):
+                span = slice(first * depth_w, (first + per_dot) * depth_w)
+                added = jnp.dot(gated, columns(first), preferred_element_type=jnp.float32)
+                current[:, span] = (current[:, span] + added).astype(jnp.bfloat16).astype(jnp.float32)
+        else:
+            mine = sp // tp
+            for j in range(0, mine, per_dot):
+                added = jnp.dot(gated, columns(t * mine + j), preferred_element_type=jnp.float32)
+                place = pl.multiple_of(t * feats + j * depth_w, depth_w)
+                total = current[:, pl.ds(place, per_dot * depth_w)] + added
+                total = total.reshape(seqs, HALO + length, per_dot * depth_w)[:, HALO:, :]
+                mixed_ref[:, :, j * depth_w : (j + per_dot) * depth_w] = total.astype(jnp.bfloat16)
+    for copy in sends:
+        copy.wait_send()
+
+
+def fused(sp, tp, sequence, norm_gain, weight_value, weight_outer, weight_inner, conv_taps, weight_out):
+    seqs, length, feats = sequence.shape
+    layers, depth_w, channels = weight_value.shape
+    rows = seqs * (HALO + length)
+    chips = sp // CORES
+    vmem = pl.BlockSpec(memory_space=pltpu.VMEM)
+    hbm = pl.BlockSpec(memory_space=pl.ANY)
+    dma = pltpu.SemaphoreType.DMA
+    return pl.pallas_call(
+        functools.partial(kernel, sp, tp),
+        out_shape=jax.ShapeDtypeStruct(sequence.shape, sequence.dtype),
+        in_specs=[hbm, vmem, hbm, hbm, hbm, vmem, hbm],
+        out_specs=vmem,
+        scratch_shapes=[
+            pltpu.VMEM((tp, seqs, length, feats), jnp.bfloat16),
+            pltpu.VMEM((tp, seqs, HALO_SENT, feats), jnp.bfloat16),
+            pltpu.VMEM((layers, sp, 3, depth_w, channels), jnp.bfloat16),
+            pltpu.VMEM((layers, sp, tp, channels, depth_w), jnp.bfloat16),
+            pltpu.VMEM((layers, tp, rows, channels), jnp.bfloat16),
+            pltpu.VMEM((rows, feats * tp), jnp.float32),
+            dma((COPIES,)),
+            dma((1 + 4 * layers,)),
+            dma((tp,)),
+            dma((tp,)),
+            dma((layers, chips, 3)),
+            dma((layers, 3)),
+            dma((layers, chips)),
+            dma((layers, tp)),
+            dma((layers, chips)),
+            dma((layers,)),
+            dma((layers, chips)),
+            dma((layers, tp)),
+        ],
+        compiler_params=pltpu.CompilerParams(collective_id=0, has_side_effects=True),
+    )(sequence, norm_gain, weight_value, weight_outer, weight_inner, conv_taps, weight_out)
+
+
+def fits(sp, tp, sequence, weight_value, conv_taps, weight_out):
+    length, feats = sequence.shape[1:]
+    depth_w, channels = weight_value.shape[1:]
+    reach = conv_taps.shape[0] * (conv_taps.shape[1] - 1)
+    aligned = feats % 128 == 0 and depth_w % 128 == 0 and channels % 128 == 0
+    shared = sp % (CORES * tp) == 0 and length % 16 == 0 and length >= HALO_SENT
+    return aligned and shared and reach <= HALO and weight_out.shape[2] == depth_w
+
+
+def either(sp, tp, sequence, norm_gain, weight_value, weight_outer, weight_inner, conv_taps, weight_out):
+    args = (sequence, norm_gain, weight_value, weight_outer, weight_inner, conv_taps, weight_out)
+    if fits(sp, tp, sequence, weight_value, conv_taps, weight_out):
+        return fused(sp, tp, *args)
+    return body(*args)
+
+
 def solution(mesh):
     return jax.shard_map(
-        body,
+        functools.partial(either, mesh.shape["sp"], mesh.shape["tp"]),
         mesh=mesh,
         in_specs=(
             P(None, "sp", "tp"),

time: 211 us -> 54.8 us (0.26)
  blocking collectives: 155 us -> 0 us
  Pallas kernels: 0 us -> 53 us
  waiting for transfers between devices: 25.8 us -> 0 us
  between operations: 13.3 us -> 0.01 us
  starting transfers between devices: 4.92 us -> 0 us
  matrix products: 4.74 us -> 0 us
  other arithmetic: 4.12 us -> 0 us
    all_gather x15 -> x0, blocking collectives: 155 us -> none  [the longest x9 82.6 us: folded(): lax.all_gather(part, axis, axis=dim, tiled=True)]
    pallas_call x0 -> x1, Pallas kernels: none -> 53 us  [fused(): pl.pallas_call(functools.partial(kernel, sp, tp), out_shape=jax.ShapeDtyp...]
    reduce_scatter x3 -> x0, waiting for transfers between devices: 24.6 us -> none  [body(): lax.psum_scatter(terms.astype(jnp.bfloat16), 'tp', scatter_dimension=1, t...]
    ppermute x3 -> x0, starting transfers between devices: 4.83 us -> none  [from_behind(): lax.ppermute(value, axis, [(source, source + steps) for source in range(f...]
    dot_general x12 -> x0, matrix products: 4.74 us -> none  [the longest x3 2.76 us: project_columns(): return jnp.dot(gated_rows, weight_cols, preferred_element_type=jnp.float32)]
    convert_element_type x9 -> x0, other arithmetic: 3.71 us -> none  [the longest x3 3.2 us: body(): current = (current.astype(jnp.float32) + shares).astype(jnp.bfloat16)]
  transfers between devices with their start and end apart: 6 -> 0, of which waited for: 3 -> 0; matrix products, arithmetic and copies ran while one was open for 0% -> 0% of each run, Pallas kernels for 0% -> 0%
where the time goes in v1:
time: 54.8 us; the launch traced here: 54.5 us
  Pallas kernels  53 us (97%)
  local copies, waits for them, and re-layouts  1.47 us (3%)
    pallas_call x1, Pallas kernels, fused(): pl.pallas_call(functools.partial(kernel, sp, tp), out_shape=jax.ShapeDtyp...  53 us
    unnamed x1, local copies, waits for them, and re-layouts  1.47 us

profile of v1, /device:TPU:0, one launch (start us, length us, event | category | flops | bytes accessed | tf_op | source)
XLA Modules:
  0.0 54.5 jit_solution(17423617304610851857)
XLA Ops:
  0.0 53.0 %shard_map.73 = bf16[4,32,256]{2,1,0:T(8,128)(2,1)} custom-call(bf16[4,32,256]{2,1,0:T(8,128)(2,1)} %seq_ref.1, f32[3,1024]{1,0:T(4,128)} %gain_ref.1, bf16[3,128,128]{2,1,0:T(8,128)(2,1)} %value_ref.1, bf16[3,128,128]{2,1,0:T(8,128)(2,1)} %outer_ref.1, bf16[3,128,128]{2,1,0:T(8,128)(2,1)} %inner_ref.1, f32[3,3,128]{2,1,0:T(4,128)} %taps_ref.1, ...), custom_call_target="tpu_custom_call" | custom-call | tf_op jit(solution)/shard_map/pallas_call | solution.py:291
  53.0 1.5 %copy.9 = bf16[4,32,256]{2,1,0:T(8,128)(2,1)} copy(bf16[4,32,256]{2,1,0:T(8,128)(2,1)} %shard_map.73) | data formatting | bytes 131072

commit v2 on v1

--- a/solution.py
+++ b/solution.py
@@ -107,6 +107,17 @@
     width = feats * tp
     sources = (value_ref, outer_ref, inner_ref)
     sends, locals_ = [], []
+    mine = sp // tp
+    goal = s // mine
+
+    def wanted(l, device):
+        return None if l < layers - 1 else device // mine == t
+
+    def only(condition, act):
+        if condition is None:
+            act()
+        else:
+            pl.when(condition)(act)
 
     def at(sp_index, tp_index):
         return {"sp": sp_index, "tp": tp_index}
@@ -117,19 +128,20 @@
     def peer(step):
         return lax.rem(chip + step + chips, chips) * CORES + core
 
-    def remote(src, dst, recv, device):
+    def remote(src, dst, recv, device, condition=None):
         copy = pltpu.make_async_remote_copy(
             src_ref=src, dst_ref=dst, send_sem=send_sem.at[len(sends)], recv_sem=recv,
             device_id=device, device_id_type=MESH,
         )
-        copy.start()
-        sends.append(copy)
-
-    def arrived(dst, recv):
-        pltpu.make_async_remote_copy(
+        only(condition, copy.start)
+        sends.append((condition, copy))
+
+    def arrived(dst, recv, condition=None):
+        copy = pltpu.make_async_remote_copy(
             src_ref=dst, dst_ref=dst, send_sem=send_sem.at[0], recv_sem=recv,
             device_id=at(partner, t), device_id_type=MESH,
-        ).wait_recv()
+        )
+        only(condition, copy.wait_recv)
 
     def local(src, dst):
         copy = pltpu.make_async_copy(src, dst, local_sem.at[len(locals_)])
@@ -158,7 +170,10 @@
 
     def send_rows(l):
         for step in range(1, tp):
-            remote(out_w_ref.at[l], wout.at[l, s, t], rows_sem.at[l, step], at(s, along(step)))
+            condition = None if l < layers - 1 else along(step) == goal
+            remote(
+                out_w_ref.at[l], wout.at[l, s, t], rows_sem.at[l, step], at(s, along(step)), condition
+            )
 
     def forward_in(l):
         for step in range(1, chips):
@@ -170,16 +185,21 @@
     def spread_out(l):
         own_out[l].wait()
         for step in range(1, tp):
-            arrived(wout.at[l, s, along(-step)], rows_sem.at[l, step])
-        for step in range(1, chips):
-            remote(wout.at[l, s], wout.at[l, s], wout_sem.at[l, step], at(peer(step), t))
-        remote(wout.at[l, s], wout.at[l, s], wout_own_sem.at[l], at(partner, t))
+            arrived(wout.at[l, s, along(-step)], rows_sem.at[l, step], wanted(l, s))
+        for step in range(1, chips):
+            remote(
+                wout.at[l, s], wout.at[l, s], wout_sem.at[l, step], at(peer(step), t), wanted(l, s)
+            )
+        remote(wout.at[l, s], wout.at[l, s], wout_own_sem.at[l], at(partner, t), wanted(l, s))
 
     def forward_out(l):
         for step in range(1, chips):
             origin = peer(-step)
-            arrived(wout.at[l, origin], wout_sem.at[l, step])
-            remote(wout.at[l, origin], wout.at[l, origin], wout_fwd_sem.at[l, step], at(partner, t))
+            need = wanted(l, origin)
+            arrived(wout.at[l, origin], wout_sem.at[l, step], need)
+            remote(
+                wout.at[l, origin], wout.at[l, origin], wout_fwd_sem.at[l, step], at(partner, t), need
+            )
 
     def finish_in(l):
         for copy in own_in[l]:
@@ -191,10 +211,10 @@
             arrived(win.at[l, origin], win_fwd_sem.at[l, step])
 
     def finish_out(l):
-        arrived(wout.at[l, partner], wout_own_sem.at[l])
+        arrived(wout.at[l, partner], wout_own_sem.at[l], wanted(l, partner))
         for step in range(1, chips):
             origin = lax.rem(chip - step + chips, chips) * CORES + (CORES - 1 - core)
-            arrived(wout.at[l, origin], wout_fwd_sem.at[l, step])
+            arrived(wout.at[l, origin], wout_fwd_sem.at[l, step], wanted(l, origin))
 
     def gate_layer(l):
         wide = current[...]
@@ -249,11 +269,13 @@
     per_dot = 2
     for l in range(layers):
         gate_layer(l)
-        if l + 2 < layers:
-            send_in(l + 2)
+        if l == 0:
+            for later in range(2, layers):
+                send_in(later)
+            for later in range(1, layers):
+                spread_out(later)
         if l + 1 < layers:
             forward_in(l + 1)
-            spread_out(l + 1)
         forward_out(l)
         gated = all_gates(l)
         finish_out(l)
@@ -276,8 +298,8 @@
                 total = current[:, pl.ds(place, per_dot * depth_w)] + added
                 total = total.reshape(seqs, HALO + length, per_dot * depth_w)[:, HALO:, :]
                 mixed_ref[:, :, j * depth_w : (j + per_dot) * depth_w] = total.astype(jnp.bfloat16)
-    for copy in sends:
-        copy.wait_send()
+    for condition, copy in sends:
+        only(condition, copy.wait_send)
 
 
 def fused(sp, tp, sequence, norm_gain, weight_value, weight_outer, weight_inner, conv_taps, weight_out):

time: 54.8 us -> 53 us (0.967)
  Pallas kernels: 53 us -> 51.2 us
    pallas_call x1, Pallas kernels: 53 us -> 51.2 us  [fused(): pl.pallas_call(functools.partial(kernel, sp, tp), out_shape=jax.ShapeDtyp...]
where the time goes in v2:
time: 53 us; the launch traced here: 52.7 us
  Pallas kernels  51.2 us (97%)
  local copies, waits for them, and re-layouts  1.47 us (3%)
    pallas_call x1, Pallas kernels, fused(): pl.pallas_call(functools.partial(kernel, sp, tp), out_shape=jax.ShapeDtyp...  51.2 us
    unnamed x1, local copies, waits for them, and re-layouts  1.47 us

profile of v2, /device:TPU:0, one launch (start us, length us, event | category | flops | bytes accessed | tf_op | source)
XLA Modules:
  0.0 52.7 jit_solution(16661349623859880569)
XLA Ops:
  0.0 51.2 %shard_map.73 = bf16[4,32,256]{2,1,0:T(8,128)(2,1)} custom-call(bf16[4,32,256]{2,1,0:T(8,128)(2,1)} %seq_ref.1, f32[3,1024]{1,0:T(4,128)} %gain_ref.1, bf16[3,128,128]{2,1,0:T(8,128)(2,1)} %value_ref.1, bf16[3,128,128]{2,1,0:T(8,128)(2,1)} %outer_ref.1, bf16[3,128,128]{2,1,0:T(8,128)(2,1)} %inner_ref.1, f32[3,3,128]{2,1,0:T(4,128)} %taps_ref.1, ...), custom_call_target="tpu_custom_call" | custom-call | tf_op jit(solution)/shard_map/pallas_call | solution.py:313
  51.2 1.5 %copy.9 = bf16[4,32,256]{2,1,0:T(8,128)(2,1)} copy(bf16[4,32,256]{2,1,0:T(8,128)(2,1)} %shard_map.73) | data formatting | bytes 131072
